TPU v7x, 32 devices: a whole 2x2x4 slice. The times are simulated.
32 devices in a mesh: ep: 8 (over z, core), tp: 4 (over y, x).
Axes of the slice: x: 2, y: 2, z: 4, core: 2. Of those that a mesh axis runs over, the one named last changes fastest.
Arguments:
- tokens: bfloat16 [2048, 2048], P('ep'), may hold values from -6 to 6
- norm_gain: float32 [2048], replicated, may hold values from 0.1 to 1.9
- route_ids: int32 [2048, 4], P('ep'), may hold values from 0 to 15, all different within a row; in each aligned block of 256 rows (0 to 255, 256 to 511, ...) at most 96 rows name the same one
- route_weights: float32 [2048, 4], P('ep'), may hold values from 0.1 to 1
- w_gate: bfloat16 [16, 2048, 2048], P('ep', None, 'tp'), may hold values from -0.33007812 to 0.33007812
- w_up: bfloat16 [16, 2048, 2048], P('ep', None, 'tp'), may hold values from -0.33007812 to 0.33007812
- w_down: bfloat16 [16, 2048, 2048], P('ep', None, 'tp'), may hold values from -0.026489258 to 0.026489258
Outputs:
- mixed_out: bfloat16 [2048, 2048], P('ep', 'tp')
Inputs may be any that keep to these rules, and one draw needn't show every extreme that they name: `route_ids`: each token names 4 different experts. Within the tokens of one index of ep (aligned blocks of 256 tokens) no expert is named more than 96 times, a bound that some block reaches.
All inputs are finite; a program needn't handle non-finite values.
Results may differ from a plain program's by a relative error of at most 0.007.
Values may be sent and summed in bfloat16 or wider, within the bound.
A program may use at most 64 MiB of HBM per device.

v0:
```python
import jax
import jax.numpy as jnp
from jax import lax
from jax.sharding import PartitionSpec as P

swiglu_limit = 7.0
swiglu_alpha = 1.702
norm_eps = 1e-05


def clamped_units(gate_pre, up_pre):
    capped = jnp.minimum(gate_pre, swiglu_limit)
    linear = jnp.clip(up_pre, -swiglu_limit, swiglu_limit)
    return capped * jax.nn.sigmoid(swiglu_alpha * capped) * (linear + 1.0)


def expert_work(outgoing, gate_weight, up_weight, down_weight):
    received = lax.all_to_all(outgoing, "ep", split_axis=1, concat_axis=1, tiled=True)
    local_count, sources, capacity, columns = received.shape
    row_count = sources * capacity
    row_block = received.reshape(local_count, row_count, columns)
    shard_piece = lax.all_gather(row_block, "tp", axis=2, tiled=True)
    gate_sum = jnp.einsum(
        "lrd,ldf->lrf", shard_piece, gate_weight, preferred_element_type=jnp.float32
    )
    up_sum = jnp.einsum("lrd,ldf->lrf", shard_piece, up_weight, preferred_element_type=jnp.float32)
    activation = clamped_units(gate_sum, up_sum).astype(jnp.bfloat16)
    out_cols = down_weight.shape[2]
    result = jnp.einsum(
        "lrf,lfd->lrd",
        lax.all_gather(activation, "tp", axis=2, tiled=True),
        down_weight,
        preferred_element_type=jnp.float32,
    )
    result = result.astype(jnp.bfloat16).reshape(local_count, sources, capacity, out_cols)
    return lax.all_to_all(result, "ep", split_axis=1, concat_axis=1, tiled=True)


def per_device(tokens, norm_gain, route_ids, route_weights, w_gate, w_up, w_down):
    local_count = w_gate.shape[0]
    sources = lax.axis_size("ep")
    tp_count = lax.axis_size("tp")
    width = tokens.shape[1]
    columns = width // tp_count
    experts = local_count * sources
    tok_rows, top_count = route_ids.shape
    capacity = 3 * tok_rows * top_count // (2 * experts)
    values = tokens.astype(jnp.float32)
    row_mean = jnp.mean(values, axis=1, keepdims=True)
    centred = values - row_mean
    row_var = jnp.mean(centred * centred, axis=1, keepdims=True)
    offset = lax.axis_index("tp") * columns
    own_cols = lax.dynamic_slice_in_dim(centred, offset, columns, 1)
    own_gain = lax.dynamic_slice_in_dim(norm_gain, offset, columns, 0)
    normed = (own_cols * lax.rsqrt(row_var + norm_eps) * own_gain).astype(jnp.bfloat16)
    flat_ids = route_ids.reshape(-1)
    matches = (flat_ids[:, None] == jnp.arange(experts, dtype=jnp.int32)[None, :]).astype(jnp.int32)
    earlier = jnp.cumsum(matches, axis=0) - matches
    slot_index = jnp.sum(earlier * matches, axis=1)
    position = (
        flat_ids % local_count * (sources * capacity)
        + flat_ids // local_count * capacity
        + slot_index
    )
    buffer_rows = local_count * sources * capacity
    placed = (
        position.reshape(tok_rows, top_count)[:, :, None]
        == jnp.arange(buffer_rows, dtype=jnp.int32)[None, None, :]
    )
    placement_matrix = jnp.any(placed, axis=1).astype(jnp.bfloat16)
    outgoing = jnp.einsum("tp,td->pd", placement_matrix, normed, preferred_element_type=jnp.float32)
    outgoing = outgoing.astype(jnp.bfloat16).reshape(local_count, sources, capacity, columns)
    returned = jnp.concatenate(
        [
            expert_work(
                outgoing[number : number + 1],
                w_gate[number : number + 1],
                w_up[number : number + 1],
                w_down[number : number + 1],
            )
            for number in range(local_count)
        ],
        axis=0,
    )
    flat_out = returned.reshape(buffer_rows, columns)
    picked = flat_out[position].reshape(tok_rows, top_count, columns).astype(jnp.float32)
    return jnp.sum(picked * route_weights[:, :, None], axis=1).astype(jnp.bfloat16)


def solution(mesh):
    return jax.shard_map(
        per_device,
        mesh=mesh,
        in_specs=(
            P("ep", None),
            P(),
            P("ep", None),
            P("ep", None),
            P("ep", None, "tp"),
            P("ep", None, "tp"),
            P("ep", None, "tp"),
        ),
        out_specs=P("ep", "tp"),
        check_vma=False,
    )
```

profile of v0, /device:TPU:0, one launch (start us, length us, event | category | flops | bytes accessed | tf_op | source)
XLA Modules:
  0.0 269.5 jit_solution(14024327743090888040)
XLA Ops:
  6.5 0.9 copy.62
  7.4 0.1 eq.44
  7.6 0.1 eq.40
  7.7 4.5 %reduce-window.6 = s32[16,8,128]{2,1,0:T(8,128)S(1)} reduce-window(s32[16,8,128]{2,1,0:T(8,128)S(1)} %fusion.42, s32[]{:T(128)} %constant.28.clone.1), window={size=1x1x128 pad=0_0x0_0x127_0}, to_apply=%region_0.0 | reduce-window | flops 2080768 | bytes 131076 | tf_op jit(solution)/shard_map/reduce-window
  12.2 0.1 slice.50
  12.3 0.1 copy.64
  12.5 0.1 copy.65
  12.5 0.1 broadcast_add_fusion
  12.7 0.1 reduce_sum.41
  12.8 0.1 copy.66
  12.9 0.7 fusion.45
  13.6 1.7 fusion
  15.3 0.2 convert_reduce_fusion
  15.6 0.4 multiply_reduce_fusion.1
  16.0 0.8 dynamic_slice.7
  16.8 1.7 convolution_convert_fusion
  18.5 0.1 fusion.53
  18.6 27.2 %all_to_all.20 = bf16[1,8,96,512]{3,2,0,1:T(8,128)(2,1)} all-to-all(bf16[1,8,96,512]{3,2,0,1:T(8,128)(2,1)S(1)} %bitcast.82), channel_id=1, replica_groups=mesh['ep'=8,'tp'=4] {'ep'}, dimensions={1} | all-to-all | bytes 1572864 | tf_op jit(solution)/shard_map/all_to_all | solution.py:18
  45.8 0.0 all-gather.7.cloned.1.call-update
  45.8 0.0 all-gather.9.cloned.1.call-start
  45.9 24.0 %all_to_all.21 = bf16[1,8,96,512]{3,2,0,1:T(8,128)(2,1)} all-to-all(bf16[1,8,96,512]{3,2,0,1:T(8,128)(2,1)S(1)} %bitcast.81), channel_id=1, replica_groups=mesh['ep'=8,'tp'=4] {'ep'}, dimensions={1} | all-to-all | bytes 1572864 | tf_op jit(solution)/shard_map/all_to_all | solution.py:18
  69.9 0.0 all-gather.9.cloned.1.call-update
  69.9 0.0 all-gather.11.cloned.1.call-start
  70.0 18.6 %all-gather.7.cloned.1.call-done = bf16[1,768,2048]{2,1,0:T(8,128)(2,1)} async-done(((bf16[1,768,512]{2,1,0:T(8,128)(2,1)}), bf16[1,768,2048]{2,1,0:T(8,128)(2,1)}) %all-gather.7.cloned.1.call-update) | async-done | bytes 3145744 | tf_op jit(solution)/shard_map/all_gather | solution.py:22
  88.6 4.5 %fusion.7 = f32[768,512]{1,0:T(8,128)S(1)} fusion(bf16[1,768,2048]{2,1,0:T(8,128)(2,1)} %all-gather.7.cloned.1.call-done, bf16[2,2048,512]{2,1,0:T(8,128)(2,1)} %param.11), kind=kOutput, calls=%fused_computation.9 | convolution fusion | flops 1610612736 | bytes 6815744 | tf_op jit(solution)/shard_map/lrd,ldf->lrf/dot_general | solution.py:23
  93.1 0.2 copy-done.5
  93.3 3.0 %multiply_convert_fusion.1 = bf16[768,512]{1,0:T(8,128)(2,1)} fusion(f32[768,512]{1,0:T(8,128)S(1)} %fusion.7, bf16[2,2048,512]{2,1,0:T(8,128)(2,1)S(1)} %copy-done.2, bf16[1,768,2048]{2,1,0:T(8,128)(2,1)S(1)} %copy-done.5), kind=kOutput, calls=%fused_computation.32 | convolution fusion | flops 1614544896 | bytes 7602176 | tf_op jit(solution)/shard_map/lrd,ldf->lrf/dot_general | solution.py:26
  96.3 0.0 all-gather.11.cloned.1.call-update
  96.4 0.0 all-gather.13.cloned.1.call-start
  96.4 37.8 %all-gather.9.cloned.1.call-done = bf16[1,768,2048]{2,1,0:T(8,128)(2,1)} async-done(((bf16[1,768,512]{2,1,0:T(8,128)(2,1)}), bf16[1,768,2048]{2,1,0:T(8,128)(2,1)}) %all-gather.9.cloned.1.call-update) | async-done | bytes 3145744 | tf_op jit(solution)/shard_map/all_gather | solution.py:22
  134.2 4.5 %fusion.3 = f32[768,512]{1,0:T(8,128)S(1)} fusion(bf16[1,768,2048]{2,1,0:T(8,128)(2,1)} %all-gather.9.cloned.1.call-done, bf16[2,2048,512]{2,1,0:T(8,128)(2,1)} %param.11), kind=kOutput, calls=%fused_computation.5 | convolution fusion | flops 1610612736 | bytes 6815744 | tf_op jit(solution)/shard_map/lrd,ldf->lrf/dot_general | solution.py:23
  138.7 0.2 copy-done.4
  138.9 3.0 %multiply_convert_fusion = bf16[768,512]{1,0:T(8,128)(2,1)} fusion(f32[768,512]{1,0:T(8,128)S(1)} %fusion.3, bf16[2,2048,512]{2,1,0:T(8,128)(2,1)S(1)} %copy-done.3, bf16[1,768,2048]{2,1,0:T(8,128)(2,1)S(1)} %copy-done.4), kind=kOutput, calls=%fused_computation.31 | convolution fusion | flops 1614544896 | bytes 7602176 | tf_op jit(solution)/shard_map/lrd,ldf->lrf/dot_general | solution.py:26
  141.9 0.0 all-gather.13.cloned.1.call-update
  141.9 37.8 %all-gather.11.cloned.1.call-done = bf16[768,2048]{1,0:T(8,128)(2,1)} async-done(((bf16[768,512]{1,0:T(8,128)(2,1)}), bf16[768,2048]{1,0:T(8,128)(2,1)}) %all-gather.11.cloned.1.call-update) | async-done | bytes 3145744 | tf_op jit(solution)/shard_map/all_gather | solution.py:31
  179.8 5.2 %fusion.31 = bf16[768,512]{1,0:T(8,128)(2,1)} fusion(bf16[768,2048]{1,0:T(8,128)(2,1)} %all-gather.11.cloned.1.call-done, bf16[2,2048,512]{2,1,0:T(8,128)(2,1)} %param.13), kind=kOutput, calls=%fused_computation.33 | convolution fusion | flops 1611005952 | bytes 6029312 | tf_op jit(solution)/shard_map/lrf,lfd->lrd/dot_general | solution.py:29
  185.0 4.6 %all-to-all-start.1 = ((bf16[1,8,96,512]{3,2,0,1:T(8,128)(2,1)}), bf16[1,8,96,512]{3,2,0,1:T(8,128)(2,1)S(1)}, u32[]{:S(2)}, u32[]{:S(2)}) async-start(bf16[1,8,96,512]{3,2,0,1:T(8,128)(2,1)} %bitcast.10), calls=%async_computation.1 | async-start | bytes 1572864 | tf_op jit(solution)/shard_map/all_to_all | solution.py:36
  189.6 35.6 %all-gather.13.cloned.1.call-done = bf16[768,2048]{1,0:T(8,128)(2,1)} async-done(((bf16[768,512]{1,0:T(8,128)(2,1)}), bf16[768,2048]{1,0:T(8,128)(2,1)}) %all-gather.13.cloned.1.call-update) | async-done | bytes 3145744 | tf_op jit(solution)/shard_map/all_gather | solution.py:31
  225.2 5.2 %fusion.34 = bf16[768,512]{1,0:T(8,128)(2,1)} fusion(bf16[768,2048]{1,0:T(8,128)(2,1)} %all-gather.13.cloned.1.call-done, bf16[2,2048,512]{2,1,0:T(8,128)(2,1)} %param.13), kind=kOutput, calls=%fused_computation.34 | convolution fusion | flops 1611005952 | bytes 6029312 | tf_op jit(solution)/shard_map/lrf,lfd->lrd/dot_general | solution.py:29
  230.4 4.6 %all-to-all-start.3 = ((bf16[1,8,96,512]{3,2,0,1:T(8,128)(2,1)}), bf16[1,8,96,512]{3,2,0,1:T(8,128)(2,1)S(1)}, u32[]{:S(2)}, u32[]{:S(2)}) async-start(bf16[1,8,96,512]{3,2,0,1:T(8,128)(2,1)} %bitcast.19), calls=%async_computation.3 | async-start | bytes 1572864 | tf_op jit(solution)/shard_map/all_to_all | solution.py:36
  235.0 0.1 reshape.289
  235.1 0.1 copy.73
  235.3 20.6 %all-to-all-done.3 = bf16[1,8,96,512]{3,2,0,1:T(8,128)(2,1)S(1)} async-done(((bf16[1,8,96,512]{3,2,0,1:T(8,128)(2,1)}), bf16[1,8,96,512]{3,2,0,1:T(8,128)(2,1)S(1)}, u32[]{:S(2)}, u32[]{:S(2)}) %all-to-all-start.3) | async-done | bytes 786464 | tf_op jit(solution)/shard_map/all_to_all | solution.py:36
  255.9 0.1 pad_maximum_fusion
  256.1 0.1 copy.71
  256.2 4.0 %gather_fusion = bf16[1024,512]{1,0:T(8,128)(2,1)S(1)} fusion(bf16[1536,512]{1,0:T(8,128)(2,1)S(1)} %bitcast.78, s32[1024]{0:T(1024)S(1)} %broadcast_clamp_fusion), kind=kCustom, calls=%fused_computation | custom fusion | bytes 2101248 | tf_op jit(solution)/shard_map/gather | solution.py:86
  260.2 0.7 reshape.290
  260.9 2.1 multiply_reduce_fusion
  (20 shorter events, 0.2 us)
Async XLA Ops:
  6.5 8.8 %copy-start = (bf16[256,2048]{1,0:T(8,128)(2,1)S(1)}, bf16[256,2048]{1,0:T(8,128)(2,1)}, u32[]{:S(2)}) copy-start(bf16[256,2048]{1,0:T(8,128)(2,1)} %param.7) | copy-start | bytes 3145732
  6.5 82.1 %all-gather.7.cloned.1.call-start = ((), (), s32[]{:S(2)}) async-start(), calls=%async_computation.4 | async-start | bytes 3932160 | tf_op jit(solution)/shard_map/all_gather | solution.py:22
  45.8 88.4 %all-gather.9.cloned.1.call-start = ((), (), s32[]{:S(2)}) async-start(), calls=%async_computation.5 | async-start | bytes 3932160 | tf_op jit(solution)/shard_map/all_gather | solution.py:22
  69.9 109.8 %all-gather.11.cloned.1.call-start = ((), (), s32[]{:S(2)}) async-start(), calls=%async_computation.6 | async-start | bytes 3932160 | tf_op jit(solution)/shard_map/all_gather | solution.py:31
  88.6 4.5 %copy-start.2 = (bf16[2,2048,512]{2,1,0:T(8,128)(2,1)S(1)}, bf16[2,2048,512]{2,1,0:T(8,128)(2,1)}, u32[]{:S(2)}) copy-start(bf16[2,2048,512]{2,1,0:T(8,128)(2,1)} %param.12) | copy-start | bytes 12582916
  88.6 4.7 %copy-start.5 = (bf16[1,768,2048]{2,1,0:T(8,128)(2,1)S(1)}, bf16[1,768,2048]{2,1,0:T(8,128)(2,1)}, u32[]{:S(2)}) copy-start(bf16[1,768,2048]{2,1,0:T(8,128)(2,1)} %all-gather.7.cloned.1.call-done) | copy-start | bytes 9437188
  96.4 128.8 %all-gather.13.cloned.1.call-start = ((), (), s32[]{:S(2)}) async-start(), calls=%async_computation.7 | async-start | bytes 3932160 | tf_op jit(solution)/shard_map/all_gather | solution.py:31
  134.2 4.5 %copy-start.3 = (bf16[2,2048,512]{2,1,0:T(8,128)(2,1)S(1)}, bf16[2,2048,512]{2,1,0:T(8,128)(2,1)}, u32[]{:S(2)}) copy-start(bf16[2,2048,512]{2,1,0:T(8,128)(2,1)} %param.12) | copy-start | bytes 12582916
  134.2 4.7 %copy-start.4 = (bf16[1,768,2048]{2,1,0:T(8,128)(2,1)S(1)}, bf16[1,768,2048]{2,1,0:T(8,128)(2,1)}, u32[]{:S(2)}) copy-start(bf16[1,768,2048]{2,1,0:T(8,128)(2,1)} %all-gather.9.cloned.1.call-done) | copy-start | bytes 9437188
  185.0 45.4 %all-to-all-start.1 = ((bf16[1,8,96,512]{3,2,0,1:T(8,128)(2,1)}), bf16[1,8,96,512]{3,2,0,1:T(8,128)(2,1)S(1)}, u32[]{:S(2)}, u32[]{:S(2)}) async-start(bf16[1,8,96,512]{3,2,0,1:T(8,128)(2,1)} %bitcast.10), calls=%async_computation.1 | async-start | bytes 1572864 | tf_op jit(solution)/shard_map/all_to_all | solution.py:36
  189.6 45.5 %copy-start.1 = (f32[256,4]{0,1:T(4,128)S(1)}, f32[256,4]{0,1:T(4,128)}, u32[]{:S(2)}) copy-start(f32[256,4]{0,1:T(4,128)} %param.10) | copy-start | bytes 12292
  230.4 25.6 %all-to-all-start.3 = ((bf16[1,8,96,512]{3,2,0,1:T(8,128)(2,1)}), bf16[1,8,96,512]{3,2,0,1:T(8,128)(2,1)S(1)}, u32[]{:S(2)}, u32[]{:S(2)}) async-start(bf16[1,8,96,512]{3,2,0,1:T(8,128)(2,1)} %bitcast.19), calls=%async_computation.3 | async-start | bytes 1572864 | tf_op jit(solution)/shard_map/all_to_all | solution.py:36
Sparse Core Ops, SparseCore 0:
  45.9 42.6 all-gather.6
  90.4 43.6 all-gather.8
  136.0 43.6 all-gather.10
  181.4 43.6 all-gather.12
where the time goes:
time: 270 us; the launch traced here: 269 us
  waiting for transfers between devices  150 us (56%)
  blocking collectives  51.2 us (19%)
  matrix products  27 us (10%)
  between operations  13.3 us (5%)
  other arithmetic  10 us (4%)
  starting transfers between devices  9.36 us (3%)
  local copies, waits for them, and re-layouts  8.03 us (3%)
    all_gather x2, waiting for transfers between devices, expert_work(): lax.all_gather(activation, 'tp', axis=2, tiled=True)  73.4 us
    all_gather x2, waiting for transfers between devices, expert_work(): shard_piece = lax.all_gather(row_block, 'tp', axis=2, tiled=True)  56.4 us
    all_to_all x2, blocking collectives, expert_work(): lax.all_to_all(outgoing, 'ep', split_axis=1, concat_axis=1, tiled=True)  51.2 us
    all_to_all x2, waiting for transfers between devices, expert_work(): return lax.all_to_all(result, 'ep', split_axis=1, concat_axis=1, tiled=True)  20.6 us
    dot_general x2, matrix products, expert_work(): jnp.einsum('lrf,lfd->lrd', lax.all_gather(activation, 'tp', axis=2, tiled...  10.4 us
    all_to_all x2, starting transfers between devices, expert_work(): return lax.all_to_all(result, 'ep', split_axis=1, concat_axis=1, tiled=True)  9.23 us
    dot_general x2, matrix products, expert_work(): jnp.einsum('lrd,ldf->lrf', shard_piece, gate_weight, preferred_element_ty...  8.95 us
    dot_general x2, matrix products, expert_work(): jnp.einsum('lrd,ldf->lrf', shard_piece, up_weight, preferred_element_type...  5.99 us
  transfers between devices with their start and end apart: 6, of which 5 were waited for; matrix products, arithmetic and copies ran while one was open for 10% of the time, Pallas kernels for 0%

commit v1 on v0

--- a/solution.py
+++ b/solution.py
@@ -6,6 +6,12 @@
 swiglu_limit = 7.0
 swiglu_alpha = 1.702
 norm_eps = 1e-05
+
+
+def stacked_exchange(x, axis, split, join):
+    pieces = jnp.split(x, lax.axis_size(axis), axis=split)
+    arrived = lax.all_to_all(jnp.stack(pieces), axis, 0, 0)
+    return jnp.concatenate(arrived, axis=join)
 
 
 def clamped_units(gate_pre, up_pre):
@@ -33,7 +39,7 @@
         preferred_element_type=jnp.float32,
     )
     result = result.astype(jnp.bfloat16).reshape(local_count, sources, capacity, out_cols)
-    return lax.all_to_all(result, "ep", split_axis=1, concat_axis=1, tiled=True)
+    return stacked_exchange(result, "ep", 1, 1)
 
 
 def per_device(tokens, norm_gain, route_ids, route_weights, w_gate, w_up, w_down):

time: 270 us -> 274 us (1.015)
  local copies, waits for them, and re-layouts: 8.03 us -> 18.2 us
  waiting for transfers between devices: 150 us -> 146 us
    unnamed x14 -> x28, local copies, waits for them, and re-layouts: 1.54 us -> 10.5 us
    all_gather x2, waiting for transfers between devices: 73.4 us -> 69.2 us  [expert_work(): lax.all_gather(activation, 'tp', axis=2, tiled=True)]
  transfers between devices with their start and end apart: 6 -> 6, of which waited for: 5 -> 5; matrix products, arithmetic and copies ran while one was open for 10% -> 12% of each run, Pallas kernels for 0% -> 0%
where the time goes in v1:
time: 274 us
  waiting for transfers between devices  146 us (53%)
  blocking collectives  51.2 us (19%)
  matrix products  25.3 us (9%)
  local copies, waits for them, and re-layouts  18.2 us (7%)
  between operations  13.3 us (5%)
  other arithmetic  10 us (4%)
  starting transfers between devices  9.37 us (3%)
    all_gather x2, waiting for transfers between devices, expert_work(): lax.all_gather(activation, 'tp', axis=2, tiled=True)  69.2 us
    all_gather x2, waiting for transfers between devices, expert_work(): shard_piece = lax.all_gather(row_block, 'tp', axis=2, tiled=True)  56.4 us
    all_to_all x2, blocking collectives, expert_work(): lax.all_to_all(outgoing, 'ep', split_axis=1, concat_axis=1, tiled=True)  51.2 us
    all_to_all x2, waiting for transfers between devices, stacked_exchange(): arrived = lax.all_to_all(jnp.stack(pieces), axis, 0, 0)  20.6 us
    unnamed x28, local copies, waits for them, and re-layouts  10.5 us
    all_to_all x2, starting transfers between devices, stacked_exchange(): arrived = lax.all_to_all(jnp.stack(pieces), axis, 0, 0)  9.24 us
    dot_general x2, matrix products, expert_work(): jnp.einsum('lrd,ldf->lrf', shard_piece, gate_weight, preferred_element_ty...  8.95 us
    dot_general x2, matrix products, expert_work(): jnp.einsum('lrf,lfd->lrd', lax.all_gather(activation, 'tp', axis=2, tiled...  8.64 us
  transfers between devices with their start and end apart: 6, of which 5 were waited for; matrix products, arithmetic and copies ran while one was open for 12% of the time, Pallas kernels for 0%

profile of v1, /device:TPU:0, one launch (start us, length us, event | category | flops | bytes accessed | tf_op | source)
XLA Modules:
  0.0 273.6 jit_solution(14410275814470723757)
XLA Ops:
  6.5 0.9 copy.92
  7.7 4.5 %reduce-window.6 = s32[16,8,128]{2,1,0:T(8,128)S(1)} reduce-window(s32[16,8,128]{2,1,0:T(8,128)S(1)} %fusion.58, s32[]{:T(128)} %constant.28.clone.1), window={size=1x1x128 pad=0_0x0_0x127_0}, to_apply=%region_0.0 | reduce-window | flops 2080768 | bytes 131076 | tf_op jit(solution)/shard_map/reduce-window
  12.3 0.1 copy.94
  12.7 0.1 reduce_sum.41
  12.9 0.7 fusion.61
  13.6 1.7 fusion
  15.3 0.2 convert_reduce_fusion
  15.6 0.4 multiply_reduce_fusion.1
  16.0 0.8 dynamic_slice.7
  16.8 1.7 convolution_convert_fusion
  18.6 27.2 %all_to_all.20 = bf16[1,8,96,512]{3,2,0,1:T(8,128)(2,1)} all-to-all(bf16[1,8,96,512]{3,2,0,1:T(8,128)(2,1)S(1)} %bitcast.146), channel_id=1, replica_groups=mesh['ep'=8,'tp'=4] {'ep'}, dimensions={1} | all-to-all | bytes 1572864 | tf_op jit(solution)/shard_map/all_to_all | solution.py:24
  45.9 24.0 %all_to_all.21 = bf16[1,8,96,512]{3,2,0,1:T(8,128)(2,1)} all-to-all(bf16[1,8,96,512]{3,2,0,1:T(8,128)(2,1)S(1)} %bitcast.145), channel_id=1, replica_groups=mesh['ep'=8,'tp'=4] {'ep'}, dimensions={1} | all-to-all | bytes 1572864 | tf_op jit(solution)/shard_map/all_to_all | solution.py:24
  70.0 18.6 %all-gather.7.cloned.1.call-done = bf16[1,768,2048]{2,1,0:T(8,128)(2,1)} async-done(((bf16[1,768,512]{2,1,0:T(8,128)(2,1)}), bf16[1,768,2048]{2,1,0:T(8,128)(2,1)}) %all-gather.7.cloned.1.call-update) | async-done | bytes 3145744 | tf_op jit(solution)/shard_map/all_gather | solution.py:28
  88.6 4.5 %fusion.7 = f32[768,512]{1,0:T(8,128)S(1)} fusion(bf16[1,768,2048]{2,1,0:T(8,128)(2,1)} %all-gather.7.cloned.1.call-done, bf16[2,2048,512]{2,1,0:T(8,128)(2,1)} %param.11), kind=kOutput, calls=%fused_computation.9 | convolution fusion | flops 1610612736 | bytes 6815744 | tf_op jit(solution)/shard_map/lrd,ldf->lrf/dot_general | solution.py:29
  93.1 0.2 copy-done.5
  93.3 3.0 %multiply_convert_fusion.1 = bf16[768,512]{1,0:T(8,128)(2,1)} fusion(f32[768,512]{1,0:T(8,128)S(1)} %fusion.7, bf16[2,2048,512]{2,1,0:T(8,128)(2,1)S(1)} %copy-done.2, bf16[1,768,2048]{2,1,0:T(8,128)(2,1)S(1)} %copy-done.5), kind=kOutput, calls=%fused_computation.32 | convolution fusion | flops 1614544896 | bytes 7602176 | tf_op jit(solution)/shard_map/lrd,ldf->lrf/dot_general | solution.py:32
  96.4 37.8 %all-gather.9.cloned.1.call-done = bf16[1,768,2048]{2,1,0:T(8,128)(2,1)} async-done(((bf16[1,768,512]{2,1,0:T(8,128)(2,1)}), bf16[1,768,2048]{2,1,0:T(8,128)(2,1)}) %all-gather.9.cloned.1.call-update) | async-done | bytes 3145744 | tf_op jit(solution)/shard_map/all_gather | solution.py:28
  134.2 4.5 %fusion.3 = f32[768,512]{1,0:T(8,128)S(1)} fusion(bf16[1,768,2048]{2,1,0:T(8,128)(2,1)} %all-gather.9.cloned.1.call-done, bf16[2,2048,512]{2,1,0:T(8,128)(2,1)} %param.11), kind=kOutput, calls=%fused_computation.5 | convolution fusion | flops 1610612736 | bytes 6815744 | tf_op jit(solution)/shard_map/lrd,ldf->lrf/dot_general | solution.py:29
  138.7 0.2 copy-done.4
  138.9 3.0 %multiply_convert_fusion = bf16[768,512]{1,0:T(8,128)(2,1)} fusion(f32[768,512]{1,0:T(8,128)S(1)} %fusion.3, bf16[2,2048,512]{2,1,0:T(8,128)(2,1)S(1)} %copy-done.3, bf16[1,768,2048]{2,1,0:T(8,128)(2,1)S(1)} %copy-done.4), kind=kOutput, calls=%fused_computation.31 | convolution fusion | flops 1614544896 | bytes 7602176 | tf_op jit(solution)/shard_map/lrd,ldf->lrf/dot_general | solution.py:32
  141.9 37.8 %all-gather.11.cloned.1.call-done = bf16[768,2048]{1,0:T(8,128)(2,1)} async-done(((bf16[768,512]{1,0:T(8,128)(2,1)}), bf16[768,2048]{1,0:T(8,128)(2,1)}) %all-gather.11.cloned.1.call-update) | async-done | bytes 3145744 | tf_op jit(solution)/shard_map/all_gather | solution.py:37
  179.8 4.3 %fusion.31 = bf16[768,512]{1,0:T(8,128)(2,1)S(1)} fusion(bf16[768,2048]{1,0:T(8,128)(2,1)} %all-gather.11.cloned.1.call-done, bf16[2,2048,512]{2,1,0:T(8,128)(2,1)} %param.13), kind=kOutput, calls=%fused_computation.33 | convolution fusion | flops 1611005952 | bytes 6029312 | tf_op jit(solution)/shard_map/lrf,lfd->lrd/dot_general | solution.py:35
  184.1 0.6 fusion.54
  184.7 0.6 fusion.53
  185.4 0.6 fusion.52
  186.0 0.6 fusion.51
  186.6 0.6 fusion.50
  187.3 0.6 fusion.49
  187.9 0.6 fusion.48
  188.6 0.6 fusion.47
  189.2 4.6 %all-to-all-start.1 = ((bf16[8,1,1,96,512]{4,3,2,1,0:T(8,128)(2,1)}), bf16[8,1,1,96,512]{4,3,2,1,0:T(8,128)(2,1)S(1)}, u32[]{:S(2)}, u32[]{:S(2)}) async-start(bf16[8,1,1,96,512]{4,3,2,1,0:T(8,128)(2,1)} %fusion.47), calls=%async_computation.1 | async-start | bytes 1572864 | tf_op jit(solution)/shard_map/all_to_all | solution.py:13
  193.8 31.4 %all-gather.13.cloned.1.call-done = bf16[768,2048]{1,0:T(8,128)(2,1)} async-done(((bf16[768,512]{1,0:T(8,128)(2,1)}), bf16[768,2048]{1,0:T(8,128)(2,1)}) %all-gather.13.cloned.1.call-update) | async-done | bytes 3145744 | tf_op jit(solution)/shard_map/all_gather | solution.py:37
  225.2 4.3 %fusion.34 = bf16[768,512]{1,0:T(8,128)(2,1)S(1)} fusion(bf16[768,2048]{1,0:T(8,128)(2,1)} %all-gather.13.cloned.1.call-done, bf16[2,2048,512]{2,1,0:T(8,128)(2,1)} %param.13), kind=kOutput, calls=%fused_computation.34 | convolution fusion | flops 1611005952 | bytes 6029312 | tf_op jit(solution)/shard_map/lrf,lfd->lrd/dot_general | solution.py:35
  229.5 0.6 fusion.46
  230.1 0.6 fusion.45
  230.8 0.6 fusion.44
  231.4 0.6 fusion.43
  232.1 0.6 fusion.42
  232.7 0.6 fusion.41
  233.4 0.6 fusion.40
  234.0 0.6 fusion.39
  234.7 4.6 %all-to-all-start.3 = ((bf16[8,1,1,96,512]{4,3,2,1,0:T(8,128)(2,1)}), bf16[8,1,1,96,512]{4,3,2,1,0:T(8,128)(2,1)S(1)}, u32[]{:S(2)}, u32[]{:S(2)}) async-start(bf16[8,1,1,96,512]{4,3,2,1,0:T(8,128)(2,1)} %fusion.39), calls=%async_computation.3 | async-start | bytes 1572864 | tf_op jit(solution)/shard_map/all_to_all | solution.py:13
  239.4 0.1 copy.100
  239.6 20.6 %all-to-all-done.3 = bf16[8,1,1,96,512]{4,3,2,1,0:T(8,128)(2,1)S(1)} async-done(((bf16[8,1,1,96,512]{4,3,2,1,0:T(8,128)(2,1)}), bf16[8,1,1,96,512]{4,3,2,1,0:T(8,128)(2,1)S(1)}, u32[]{:S(2)}, u32[]{:S(2)}) %all-to-all-start.3) | async-done | bytes 786464 | tf_op jit(solution)/shard_map/all_to_all | solution.py:13
  260.2 0.1 pad_maximum_fusion
  260.4 4.0 %gather_fusion = bf16[1024,512]{1,0:T(8,128)(2,1)S(1)} fusion(bf16[1536,512]{1,0:T(8,128)(2,1)S(1)} %bitcast.140, s32[1024]{0:T(1024)S(1)} %broadcast_clamp_fusion), kind=kCustom, calls=%fused_computation | custom fusion | bytes 2101248 | tf_op jit(solution)/shard_map/gather | solution.py:92
  264.3 0.7 reshape.298
  265.0 2.1 multiply_reduce_fusion
  (35 shorter events, 1.1 us)
Async XLA Ops:
  6.5 8.8 %copy-start = (bf16[256,2048]{1,0:T(8,128)(2,1)S(1)}, bf16[256,2048]{1,0:T(8,128)(2,1)}, u32[]{:S(2)}) copy-start(bf16[256,2048]{1,0:T(8,128)(2,1)} %param.7) | copy-start | bytes 3145732
  6.5 82.1 %all-gather.7.cloned.1.call-start = ((), (), s32[]{:S(2)}) async-start(), calls=%async_computation.4 | async-start | bytes 3932160 | tf_op jit(solution)/shard_map/all_gather | solution.py:28
  45.8 88.4 %all-gather.9.cloned.1.call-start = ((), (), s32[]{:S(2)}) async-start(), calls=%async_computation.5 | async-start | bytes 3932160 | tf_op jit(solution)/shard_map/all_gather | solution.py:28
  69.9 109.8 %all-gather.11.cloned.1.call-start = ((), (), s32[]{:S(2)}) async-start(), calls=%async_computation.6 | async-start | bytes 3932160 | tf_op jit(solution)/shard_map/all_gather | solution.py:37
  88.6 4.5 %copy-start.2 = (bf16[2,2048,512]{2,1,0:T(8,128)(2,1)S(1)}, bf16[2,2048,512]{2,1,0:T(8,128)(2,1)}, u32[]{:S(2)}) copy-start(bf16[2,2048,512]{2,1,0:T(8,128)(2,1)} %param.12) | copy-start | bytes 12582916
  88.6 4.7 %copy-start.5 = (bf16[1,768,2048]{2,1,0:T(8,128)(2,1)S(1)}, bf16[1,768,2048]{2,1,0:T(8,128)(2,1)}, u32[]{:S(2)}) copy-start(bf16[1,768,2048]{2,1,0:T(8,128)(2,1)} %all-gather.7.cloned.1.call-done) | copy-start | bytes 9437188
  96.4 128.8 %all-gather.13.cloned.1.call-start = ((), (), s32[]{:S(2)}) async-start(), calls=%async_computation.7 | async-start | bytes 3932160 | tf_op jit(solution)/shard_map/all_gather | solution.py:37
  134.2 4.5 %copy-start.3 = (bf16[2,2048,512]{2,1,0:T(8,128)(2,1)S(1)}, bf16[2,2048,512]{2,1,0:T(8,128)(2,1)}, u32[]{:S(2)}) copy-start(bf16[2,2048,512]{2,1,0:T(8,128)(2,1)} %param.12) | copy-start | bytes 12582916
  134.2 4.7 %copy-start.4 = (bf16[1,768,2048]{2,1,0:T(8,128)(2,1)S(1)}, bf16[1,768,2048]{2,1,0:T(8,128)(2,1)}, u32[]{:S(2)}) copy-start(bf16[1,768,2048]{2,1,0:T(8,128)(2,1)} %all-gather.9.cloned.1.call-done) | copy-start | bytes 9437188
  189.2 45.5 %all-to-all-start.1 = ((bf16[8,1,1,96,512]{4,3,2,1,0:T(8,128)(2,1)}), bf16[8,1,1,96,512]{4,3,2,1,0:T(8,128)(2,1)S(1)}, u32[]{:S(2)}, u32[]{:S(2)}) async-start(bf16[8,1,1,96,512]{4,3,2,1,0:T(8,128)(2,1)} %fusion.47), calls=%async_computation.1 | async-start | bytes 1572864 | tf_op jit(solution)/shard_map/all_to_all | solution.py:13
  229.5 9.9 %copy-start.1 = (f32[256,4]{0,1:T(4,128)S(1)}, f32[256,4]{0,1:T(4,128)}, u32[]{:S(2)}) copy-start(f32[256,4]{0,1:T(4,128)} %param.10) | copy-start | bytes 12292
  234.7 25.6 %all-to-all-start.3 = ((bf16[8,1,1,96,512]{4,3,2,1,0:T(8,128)(2,1)}), bf16[8,1,1,96,512]{4,3,2,1,0:T(8,128)(2,1)S(1)}, u32[]{:S(2)}, u32[]{:S(2)}) async-start(bf16[8,1,1,96,512]{4,3,2,1,0:T(8,128)(2,1)} %fusion.39), calls=%async_computation.3 | async-start | bytes 1572864 | tf_op jit(solution)/shard_map/all_to_all | solution.py:13
Sparse Core Ops, SparseCore 0:
  45.9 42.6 all-gather.6
  90.4 43.6 all-gather.8
  136.0 43.7 all-gather.10
  181.4 43.6 all-gather.12
